TPU v7x, 32 devices: a whole 2x2x4 slice. The times are simulated.
32 devices in a mesh: sp: 8 (over z, y), tp: 4 (over x, core).
Axes of the slice: x: 2, y: 2, z: 4, core: 2. Of those that a mesh axis runs over, the one named last changes fastest.
Arguments:
- latents: bfloat16 [2048, 4096], P('sp'), may hold values from -0.4375 to 0.4375
- query_heads: bfloat16 [2048, 16, 128], P('sp', 'tp'), may hold values from -8 to 8
- key_heads: bfloat16 [2048, 16, 128], P('sp', 'tp'), may hold values from -8 to 8
- value_heads: bfloat16 [2048, 16, 128], P('sp', 'tp'), may hold values from -6 to 6
- map_outputs: bfloat16 [2048, 2, 16, 128], P('sp', None, 'tp'), may hold values from -6 to 6
- log_sums: float32 [2048, 16, 2], P('sp', 'tp'), may hold values from -600 to 600, as said below
- out_grad: bfloat16 [2048, 16, 128], P('sp', 'tp'), may hold values from -6 to 6
- mix_lambda: float32 [16], P('tp'), may hold values from 0.3 to 0.8
- norm_gain: float32 [128], replicated, may hold values from 0.1 to 1.9
Outputs:
- query_grad: bfloat16 [2048, 16, 128], P('sp', 'tp')
- key_grad: bfloat16 [2048, 16, 128], P('sp', 'tp')
- value_grad: bfloat16 [2048, 16, 128], P('sp', 'tp')
- weight_grad: float32 [4096, 2048], P('sp', 'tp')
Inputs may be any that keep to these rules, and one draw needn't show every extreme that they name: query_heads, key_heads and value_heads together with map_outputs and log_sums are one consistent causal forward pass: log_sums is the row's log-sum of exp(score_m) over keys at or before the row, and map_outputs[:, m] is prob_m times value_heads rounded to bfloat16.
All inputs are finite; a program needn't handle non-finite values.
Results may differ from a plain program's by a relative error of at most 0.019.
Values may be sent and summed in bfloat16 or wider, within the bound.
A program may use at most 64 MiB of HBM per device.

v0:
```python
import jax
import jax.numpy as jnp
from jax import lax
from jax.sharding import PartitionSpec as P

DH = 64


EPSILON = 1e-05


def norm_backward(map_outputs, out_grad, mix_lambda, norm_gain):
    first_map = map_outputs[:, 0].astype(jnp.float32)
    second_map = map_outputs[:, 1].astype(jnp.float32)
    lambda_col = mix_lambda[None, :, None]
    combined = first_map - lambda_col * second_map
    inverse = lax.rsqrt(jnp.mean(combined * combined, axis=-1, keepdims=True) + EPSILON)
    weighted = norm_gain[None, None, :] * out_grad.astype(jnp.float32)
    grad_out = (
        inverse * weighted
        - inverse**3 * combined * jnp.mean(combined * weighted, axis=-1, keepdims=True)
    ).astype(jnp.bfloat16)
    grad_wide = grad_out.astype(jnp.float32)
    row_terms = jnp.stack(
        [jnp.sum(grad_wide * first_map, axis=-1), jnp.sum(grad_wide * second_map, axis=-1)], axis=-1
    )
    return (grad_out, row_terms)


def block_grads(
    query_blk, grad_blk, lse_blk, term_blk, key_blk, value_blk, query_pos, key_pos, mix_lambda
):
    row_count = query_blk.shape[0]
    col_count = key_blk.shape[0]
    head_count = query_blk.shape[1]
    score_scale = DH ** (-0.5)
    query_split = query_blk.reshape(row_count, head_count, 2, DH)
    key_split = key_blk.reshape(col_count, head_count, 2, DH)
    scores = (
        jnp.einsum("qhmd,khmd->hmqk", query_split, key_split, preferred_element_type=jnp.float32)
        * score_scale
    )
    causal = key_pos[None, :] <= query_pos[:, None]
    softmax_maps = jnp.exp(
        jnp.where(causal, scores - jnp.transpose(lse_blk, (1, 2, 0))[..., None], -jnp.inf)
    )
    mixed_grad = jnp.einsum("qhe,khe->hqk", grad_blk, value_blk, preferred_element_type=jnp.float32)
    map_signs = jnp.stack([jnp.ones_like(mix_lambda), -mix_lambda], axis=1)[:, :, None, None]
    score_grad = (
        map_signs
        * softmax_maps
        * (mixed_grad[:, None] - jnp.transpose(term_blk, (1, 2, 0))[..., None])
    ).astype(jnp.bfloat16)
    diff_weights = (softmax_maps[:, 0] - mix_lambda[:, None, None] * softmax_maps[:, 1]).astype(
        jnp.bfloat16
    )
    value_part = jnp.einsum(
        "hqk,qhe->khe", diff_weights, grad_blk, preferred_element_type=jnp.float32
    )
    query_part = score_scale * jnp.einsum(
        "hmqk,khmd->qhmd", score_grad, key_split, preferred_element_type=jnp.float32
    )
    key_part = score_scale * jnp.einsum(
        "hmqk,qhmd->khmd", score_grad, query_split, preferred_element_type=jnp.float32
    )
    return (
        query_part.reshape(row_count, head_count, 2 * DH),
        key_part.reshape(col_count, head_count, 2 * DH),
        value_part,
    )


def unchanged(running):
    return running


def body(
    latents,
    query_heads,
    key_heads,
    value_heads,
    map_outputs,
    log_sums,
    out_grad,
    mix_lambda,
    norm_gain,
):
    rows_dev = query_heads.shape[0]
    head_count = query_heads.shape[1]
    width = query_heads.shape[2]
    offset = lax.axis_index("sp") * rows_dev
    own_pos = offset + jnp.arange(rows_dev, dtype=jnp.int32)
    grad_out, row_terms = norm_backward(map_outputs, out_grad, mix_lambda, norm_gain)
    local_zero = jnp.zeros((rows_dev, head_count, width), jnp.float32)
    row_stats = jnp.concatenate([log_sums, row_terms], axis=-1)
    all_stats = lax.all_gather(row_stats, "sp", axis=0, tiled=True)
    key_piece = lax.all_gather(key_heads, "sp", axis=0, tiled=True)
    value_piece = lax.all_gather(value_heads, "sp", axis=0, tiled=True)
    pieces = key_piece.shape[0] // rows_dev
    blocks = (
        key_piece.reshape(pieces, rows_dev, head_count, width),
        value_piece.reshape(pieces, rows_dev, head_count, width),
        jnp.arange(pieces, dtype=jnp.int32),
    )

    def visit(state, element):
        key_blk, value_blk, block_index = element
        first_key = block_index * rows_dev

        def accumulate(query_acc):
            key_pos = first_key + jnp.arange(rows_dev, dtype=jnp.int32)
            query_part, _, _ = block_grads(
                query_heads,
                grad_out,
                log_sums,
                row_terms,
                key_blk,
                value_blk,
                own_pos,
                key_pos,
                mix_lambda,
            )
            return query_acc + query_part

        return (lax.cond(first_key < offset + rows_dev, accumulate, unchanged, state), None)

    result, _ = lax.scan(visit, local_zero, blocks)
    query_acc = result
    query_piece = lax.all_gather(query_heads, "sp", axis=0, tiled=True)
    grad_piece = lax.all_gather(grad_out, "sp", axis=0, tiled=True)
    pieces = query_piece.shape[0] // rows_dev
    blocks = (
        query_piece.reshape(pieces, rows_dev, head_count, width),
        grad_piece.reshape(pieces, rows_dev, head_count, width),
        jnp.arange(pieces, dtype=jnp.int32),
    )

    def visit(state, element):
        query_blk, grad_blk, block_index = element
        first_query = block_index * rows_dev

        def accumulate(inner):
            key_acc, value_acc = inner
            query_pos = first_query + jnp.arange(rows_dev, dtype=jnp.int32)
            stats_blk = lax.dynamic_slice_in_dim(all_stats, first_query, rows_dev, 0)
            _, key_part, value_part = block_grads(
                query_blk,
                grad_blk,
                stats_blk[..., :2],
                stats_blk[..., 2:],
                key_heads,
                value_heads,
                query_pos,
                own_pos,
                mix_lambda,
            )
            return (key_acc + key_part, value_acc + value_part)

        return (lax.cond(first_query + rows_dev > offset, accumulate, unchanged, state), None)

    result, _ = lax.scan(visit, (local_zero, local_zero), blocks)
    key_acc, value_acc = result
    query_grad = query_acc.astype(jnp.bfloat16)
    flat_grad = query_grad.reshape(rows_dev, head_count * width)
    weight_grad = lax.psum_scatter(
        lax.dot_general(
            latents, flat_grad, (((0,), (0,)), ((), ())), preferred_element_type=jnp.float32
        ).astype(jnp.bfloat16),
        "sp",
        scatter_dimension=0,
        tiled=True,
    ).astype(jnp.float32)
    return (query_grad, key_acc.astype(jnp.bfloat16), value_acc.astype(jnp.bfloat16), weight_grad)


def solution(mesh):
    placed = (
        P("sp", None),
        P("sp", "tp", None),
        P("sp", "tp", None),
        P("sp", "tp", None),
        P("sp", None, "tp", None),
        P("sp", "tp", None),
        P("sp", "tp", None),
        P("tp"),
        P(),
    )
    return jax.shard_map(
        body,
        mesh=mesh,
        in_specs=placed,
        out_specs=(P("sp", "tp", None), P("sp", "tp", None), P("sp", "tp", None), P("sp", "tp")),
        check_vma=False,
    )
```

profile of v0, /device:TPU:0, one launch (start us, length us, event | category | flops | bytes accessed | tf_op | source)
XLA Modules:
  0.0 374.7 jit_solution(14575236369134222766)
XLA Ops:
  7.3 1.8 copy.50
  9.9 1.7 copy.58
  13.0 1.9 fusion.39
  15.9 46.7 %all-gather.5.cloned.1.call-done = bf16[2048,4,128]{2,0,1:T(8,128)(2,1)} async-done(((bf16[256,4,128]{2,0,1:T(8,128)(2,1)}), bf16[2048,4,128]{2,0,1:T(8,128)(2,1)}) %all-gather.5.cloned.1.call-update) | async-done | bytes 2097168 | tf_op jit(solution)/shard_map/all_gather | solution.py:97
  62.6 3.9 %copy.54 = bf16[8,256,4,128]{1,3,2,0:T(8,128)(2,1)} copy(bf16[8,256,4,128]{3,1,0,2:T(8,128)(2,1)} %bitcast.124) | data formatting | bytes 4194304
  66.5 45.8 %all-gather.7.cloned.1.call-done = bf16[2048,4,128]{2,1,0:T(4,128)(2,1)} async-done(((bf16[256,4,128]{2,1,0:T(4,128)(2,1)}), bf16[2048,4,128]{2,1,0:T(4,128)(2,1)}) %all-gather.7.cloned.1.call-update) | async-done | bytes 2097168 | tf_op jit(solution)/shard_map/all_gather | solution.py:98
  112.4 3.5 copy.56
  116.7 19.2 %while.30 = (s32[]{:T(128)}, f32[256,4,128]{0,2,1:T(8,128)}, s32[8]{0:T(128)S(1)}, s32[]{:T(128)}, f32[4]{0:T(128)}, /*index=5*/bf16[8,256,4,128]{1,3,2,0:T(8,12...) while((s32[]{:T(128)}, f32[256,4,128]{0,2,1:T(8,128)}, ...), condition=%wide.region_7.8_spmd.clone, body=%wide.region_4.7_spmd.clone.sunk | while | flops 205324800 | bytes 5921723 | solution.py:127
  118.0 8.9 %conditional.7 = (f32[256,4,128]{0,2,1:T(8,128)}) conditional(s32[]{:T(128)} %convert_element_type.109, f32[256,4,128]{0,2,1:T(8,128)} %get-tuple-element.780, (f32[4]{0:T(128)}, s32[]{:T(128)}, s32[]{:T(128)}, bf16[8,256,4,128]{1,3,2,0:T(8,128)(2,1)}, s32[]{:T(128)}, /*index=5*/bf16[256,4,128]{0,2,1:T(8,128)(2,1)}, f32[256,4,2]{0,2,1:T(2,128)S(1)}, ...), branch_computations={%region_5.5_spmd, %region_6.6_spmd} | conditional | flops 205324800 | bytes 5920424 | solution.py:125
  118.0 1.7 constant_dynamic-slice_fusion
  119.6 1.3 convolution_bitcast_fusion
  121.9 3.0 fusion.9
  124.8 2.1 bitcast_add_fusion
  135.9 1.3 copy.57
  137.2 3.2 fusion.38
  143.0 90.8 %all_gather.18 = f32[2048,4,4]{0,2,1:T(4,128)S(1)} all-gather(f32[256,4,4]{0,2,1:T(4,128)S(1)} %pad_maximum_fusion), channel_id=1, replica_groups=mesh['sp'=8,'tp'=4] {'sp'}, dimensions={0}, use_global_device_ids=true | all-gather | bytes 147456 | tf_op jit(solution)/shard_map/all_gather | solution.py:96
  233.9 4.0 %copy.60 = bf16[8,256,4,128]{1,3,2,0:T(8,128)(2,1)} copy(bf16[8,256,4,128]{3,1,0,2:T(8,128)(2,1)} %bitcast.122) | data formatting | bytes 4194304
  237.8 3.3 copy.62
  243.3 118.6 %while.31 = (s32[]{:T(128)}, f32[256,4,128]{0,2,1:T(8,128)}, f32[256,4,128]{2,0,1:T(8,128)}, s32[8]{0:T(128)}, s32[]{:T(128)}, /*index=5*/f32[4]{0:T(128)}, bf16...) while((s32[]{:T(128)}, f32[256,4,128]{0,2,1:T(8,128)}, ...), condition=%wide.region_11.12_spmd.clone.clone, body=%wide.region_8.11_spmd.clone.clone.sunk | while | flops 273351168 | bytes 23257172 | solution.py:161
  245.2 12.9 %conditional.8 = ((f32[256,4,128]{0,2,1:T(8,128)}, f32[256,4,128]{2,0,1:T(8,128)})) conditional(s32[]{:T(128)} %convert_element_type.110, (f32[256,4,128]{0,2,1:T(8,128)}, f32[256,4,128]{2,0,1:T(8,128)}) %tuple.101, (f32[4]{0:T(128)}, s32[]{:T(128)}, s32[]{:T(128)}, bf16[8,256,4,128]{1,3,2,0:T(8,128)(2,1)}, s32[]{:T(128)}, ...), branch_computations={%region_9.9_spmd, %region_10.10_spmd} | conditional | flops 273351168 | bytes 23255846 | solution.py:159
  246.5 3.0 select_exponential_fusion
  249.5 1.3 fusion.32
  251.6 2.3 convolution_multiply_fusion
  253.9 1.9 bitcast_add_fusion.1
  255.8 2.4 fusion.22
  260.1 12.9 %conditional.8 = ((f32[256,4,128]{0,2,1:T(8,128)}, f32[256,4,128]{2,0,1:T(8,128)})) conditional(s32[]{:T(128)} %convert_element_type.110, (f32[256,4,128]{0,2,1:T(8,128)}, f32[256,4,128]{2,0,1:T(8,128)}) %tuple.101, (f32[4]{0:T(128)}, s32[]{:T(128)}, s32[]{:T(128)}, bf16[8,256,4,128]{1,3,2,0:T(8,128)(2,1)}, s32[]{:T(128)}, ...), branch_computations={%region_9.9_spmd, %region_10.10_spmd} | conditional | flops 273351168 | bytes 23255846 | solution.py:159
  261.3 3.0 select_exponential_fusion
  264.4 1.2 fusion.32
  266.4 2.3 convolution_multiply_fusion
  268.8 1.9 bitcast_add_fusion.1
  270.6 2.4 fusion.22
  275.0 12.9 %conditional.8 = ((f32[256,4,128]{0,2,1:T(8,128)}, f32[256,4,128]{2,0,1:T(8,128)})) conditional(s32[]{:T(128)} %convert_element_type.110, (f32[256,4,128]{0,2,1:T(8,128)}, f32[256,4,128]{2,0,1:T(8,128)}) %tuple.101, (f32[4]{0:T(128)}, s32[]{:T(128)}, s32[]{:T(128)}, bf16[8,256,4,128]{1,3,2,0:T(8,128)(2,1)}, s32[]{:T(128)}, ...), branch_computations={%region_9.9_spmd, %region_10.10_spmd} | conditional | flops 273351168 | bytes 23255846 | solution.py:159
  276.2 3.0 select_exponential_fusion
  281.3 2.3 convolution_multiply_fusion
  283.6 1.9 bitcast_add_fusion.1
  285.5 2.4 fusion.22
  289.8 12.9 %conditional.8 = ((f32[256,4,128]{0,2,1:T(8,128)}, f32[256,4,128]{2,0,1:T(8,128)})) conditional(s32[]{:T(128)} %convert_element_type.110, (f32[256,4,128]{0,2,1:T(8,128)}, f32[256,4,128]{2,0,1:T(8,128)}) %tuple.101, (f32[4]{0:T(128)}, s32[]{:T(128)}, s32[]{:T(128)}, bf16[8,256,4,128]{1,3,2,0:T(8,128)(2,1)}, s32[]{:T(128)}, ...), branch_computations={%region_9.9_spmd, %region_10.10_spmd} | conditional | flops 273351168 | bytes 23255846 | solution.py:159
  291.0 3.0 select_exponential_fusion
  296.1 2.3 convolution_multiply_fusion
  298.4 1.9 bitcast_add_fusion.1
  300.3 2.4 fusion.22
  304.6 12.9 %conditional.8 = ((f32[256,4,128]{0,2,1:T(8,128)}, f32[256,4,128]{2,0,1:T(8,128)})) conditional(s32[]{:T(128)} %convert_element_type.110, (f32[256,4,128]{0,2,1:T(8,128)}, f32[256,4,128]{2,0,1:T(8,128)}) %tuple.101, (f32[4]{0:T(128)}, s32[]{:T(128)}, s32[]{:T(128)}, bf16[8,256,4,128]{1,3,2,0:T(8,128)(2,1)}, s32[]{:T(128)}, ...), branch_computations={%region_9.9_spmd, %region_10.10_spmd} | conditional | flops 273351168 | bytes 23255846 | solution.py:159
  305.9 3.0 select_exponential_fusion
  311.0 2.3 convolution_multiply_fusion
  313.2 1.9 bitcast_add_fusion.1
  315.1 2.4 fusion.22
  319.4 12.9 %conditional.8 = ((f32[256,4,128]{0,2,1:T(8,128)}, f32[256,4,128]{2,0,1:T(8,128)})) conditional(s32[]{:T(128)} %convert_element_type.110, (f32[256,4,128]{0,2,1:T(8,128)}, f32[256,4,128]{2,0,1:T(8,128)}) %tuple.101, (f32[4]{0:T(128)}, s32[]{:T(128)}, s32[]{:T(128)}, bf16[8,256,4,128]{1,3,2,0:T(8,128)(2,1)}, s32[]{:T(128)}, ...), branch_computations={%region_9.9_spmd, %region_10.10_spmd} | conditional | flops 273351168 | bytes 23255846 | solution.py:159
  320.7 3.0 select_exponential_fusion
  325.8 2.3 convolution_multiply_fusion
  328.0 1.9 bitcast_add_fusion.1
  329.9 2.4 fusion.22
  334.2 12.9 %conditional.8 = ((f32[256,4,128]{0,2,1:T(8,128)}, f32[256,4,128]{2,0,1:T(8,128)})) conditional(s32[]{:T(128)} %convert_element_type.110, (f32[256,4,128]{0,2,1:T(8,128)}, f32[256,4,128]{2,0,1:T(8,128)}) %tuple.101, (f32[4]{0:T(128)}, s32[]{:T(128)}, s32[]{:T(128)}, bf16[8,256,4,128]{1,3,2,0:T(8,128)(2,1)}, s32[]{:T(128)}, ...), branch_computations={%region_9.9_spmd, %region_10.10_spmd} | conditional | flops 273351168 | bytes 23255846 | solution.py:159
  335.5 3.0 select_exponential_fusion
  340.6 2.3 convolution_multiply_fusion
  342.8 1.9 bitcast_add_fusion.1
  344.7 2.4 fusion.22
  349.0 12.9 %conditional.8 = ((f32[256,4,128]{0,2,1:T(8,128)}, f32[256,4,128]{2,0,1:T(8,128)})) conditional(s32[]{:T(128)} %convert_element_type.110, (f32[256,4,128]{0,2,1:T(8,128)}, f32[256,4,128]{2,0,1:T(8,128)}) %tuple.101, (f32[4]{0:T(128)}, s32[]{:T(128)}, s32[]{:T(128)}, bf16[8,256,4,128]{1,3,2,0:T(8,128)(2,1)}, s32[]{:T(128)}, ...), branch_computations={%region_9.9_spmd, %region_10.10_spmd} | conditional | flops 273351168 | bytes 23255846 | solution.py:159
  350.3 3.0 select_exponential_fusion
  355.4 2.3 convolution_multiply_fusion
  357.6 1.9 bitcast_add_fusion.1
  359.5 2.4 fusion.22
  361.9 2.0 copy.64
  363.9 2.1 copy.104
  366.0 2.2 copy.66
  (186 shorter events, 47.9 us)
Async XLA Ops:
  7.2 130.0 %copy-start = (bf16[256,4096]{1,0:T(8,128)(2,1)S(1)}, bf16[256,4096]{1,0:T(8,128)(2,1)}, u32[]{:S(2)}) copy-start(bf16[256,4096]{1,0:T(8,128)(2,1)} %param.17) | copy-start | bytes 6291460
  7.2 4.5 %copy-start.9 = (bf16[256,2,4,128]{3,2,1,0:T(4,128)(2,1)S(1)}, bf16[256,2,4,128]{3,2,1,0:T(4,128)(2,1)}, u32[]{:S(2)}) copy-start(bf16[256,2,4,128]{3,2,1,0:T(4,128)(2,1)} %param.21) | copy-start | bytes 1572868
  7.2 4.7 %copy-start.5 = (bf16[256,4,128]{2,1,0:T(4,128)(2,1)S(1)}, bf16[256,4,128]{2,1,0:T(4,128)(2,1)}, u32[]{:S(2)}) copy-start(bf16[256,4,128]{2,1,0:T(4,128)(2,1)} %param.23) | copy-start | bytes 786436
  7.2 4.7 %copy-start.11 = (f32[128]{0:T(128)S(1)}, f32[128]{0:T(128)}, u32[]{:S(2)}) copy-start(f32[128]{0:T(128)} %param.25) | copy-start | bytes 1540
  7.2 55.4 %all-gather.5.cloned.1.call-start = ((), (), s32[]{:S(2)}) async-start(), calls=%async_computation.1 | async-start | bytes 2359296 | tf_op jit(solution)/shard_map/all_gather | solution.py:97
  9.1 5.9 %copy-start.6 = (bf16[256,4,128]{2,1,0:T(4,128)(2,1)S(1)}, bf16[256,4,128]{2,1,0:T(4,128)(2,1)}, u32[]{:S(2)}) copy-start(bf16[256,4,128]{2,1,0:T(4,128)(2,1)} %param.18) | copy-start | bytes 786436
  9.1 103.3 %all-gather.7.cloned.1.call-start = ((), (), s32[]{:S(2)}) async-start(), calls=%async_computation.2 | async-start | bytes 2359296 | tf_op jit(solution)/shard_map/all_gather | solution.py:98
  9.9 224.0 %all-gather.9.cloned.1.call-start = ((), (), s32[]{:S(2)}) async-start(), calls=%async_computation.3 | async-start | bytes 2359296 | tf_op jit(solution)/shard_map/all_gather | solution.py:129
  11.7 226.2 %all-gather.11.cloned.1.call-start = ((), (), s32[]{:S(2)}) async-start(), calls=%async_computation.4 | async-start | bytes 2359296 | tf_op jit(solution)/shard_map/all_gather | solution.py:130
  14.9 351.0 %reduce-scatter.2.cloned.1.call-start = ((), (), s32[]{:S(2)}) async-start(), calls=%async_computation.5 | async-start | bytes 4718592 | tf_op jit(solution)/shard_map/reduce_scatter | solution.py:165
  112.4 4.3 %copy-start.2 = (bf16[256,4,128]{2,0,1:T(8,128)(2,1)S(1)}, bf16[256,4,128]{2,0,1:T(8,128)(2,1)}, u32[]{:S(2)}) copy-start(bf16[256,4,128]{2,0,1:T(8,128)(2,1)} %get-tuple-element.774) | copy-start | bytes 786436
  112.4 4.3 %copy-start.10 = (f32[256,4,2]{0,2,1:T(2,128)S(1)}, f32[256,4,2]{0,2,1:T(2,128)}, u32[]{:S(2)}) copy-start(f32[256,4,2]{0,2,1:T(2,128)} %param.22) | copy-start | bytes 24580
  137.2 3.2 copy-start.4
  140.4 1.0 copy-start.7
  140.4 1.8 copy-start.8
  246.2 3.3 copy-start.3
  251.6 4.2 %copy-start.1 = (f32[4,2,256,256]{3,2,1,0:T(8,128)S(1)}, f32[4,2,256,256]{3,2,1,0:T(8,128)}, u32[]{:S(2)}) copy-start(f32[4,2,256,256]{3,2,1,0:T(8,128)} %select_exponential_fusion) | copy-start | bytes 6291460 | tf_op jit(solution)/shard_map/while/body/eval_jaxpr/cond
  261.1 3.3 copy-start.3
  266.4 4.2 %copy-start.1 = (f32[4,2,256,256]{3,2,1,0:T(8,128)S(1)}, f32[4,2,256,256]{3,2,1,0:T(8,128)}, u32[]{:S(2)}) copy-start(f32[4,2,256,256]{3,2,1,0:T(8,128)} %select_exponential_fusion) | copy-start | bytes 6291460 | tf_op jit(solution)/shard_map/while/body/eval_jaxpr/cond
  276.0 3.3 copy-start.3
  281.3 4.2 %copy-start.1 = (f32[4,2,256,256]{3,2,1,0:T(8,128)S(1)}, f32[4,2,256,256]{3,2,1,0:T(8,128)}, u32[]{:S(2)}) copy-start(f32[4,2,256,256]{3,2,1,0:T(8,128)} %select_exponential_fusion) | copy-start | bytes 6291460 | tf_op jit(solution)/shard_map/while/body/eval_jaxpr/cond
  290.8 3.3 copy-start.3
  296.1 4.2 %copy-start.1 = (f32[4,2,256,256]{3,2,1,0:T(8,128)S(1)}, f32[4,2,256,256]{3,2,1,0:T(8,128)}, u32[]{:S(2)}) copy-start(f32[4,2,256,256]{3,2,1,0:T(8,128)} %select_exponential_fusion) | copy-start | bytes 6291460 | tf_op jit(solution)/shard_map/while/body/eval_jaxpr/cond
  305.6 3.3 copy-start.3
  311.0 4.2 %copy-start.1 = (f32[4,2,256,256]{3,2,1,0:T(8,128)S(1)}, f32[4,2,256,256]{3,2,1,0:T(8,128)}, u32[]{:S(2)}) copy-start(f32[4,2,256,256]{3,2,1,0:T(8,128)} %select_exponential_fusion) | copy-start | bytes 6291460 | tf_op jit(solution)/shard_map/while/body/eval_jaxpr/cond
  320.4 3.3 copy-start.3
  325.8 4.2 %copy-start.1 = (f32[4,2,256,256]{3,2,1,0:T(8,128)S(1)}, f32[4,2,256,256]{3,2,1,0:T(8,128)}, u32[]{:S(2)}) copy-start(f32[4,2,256,256]{3,2,1,0:T(8,128)} %select_exponential_fusion) | copy-start | bytes 6291460 | tf_op jit(solution)/shard_map/while/body/eval_jaxpr/cond
  335.2 3.3 copy-start.3
  340.6 4.2 %copy-start.1 = (f32[4,2,256,256]{3,2,1,0:T(8,128)S(1)}, f32[4,2,256,256]{3,2,1,0:T(8,128)}, u32[]{:S(2)}) copy-start(f32[4,2,256,256]{3,2,1,0:T(8,128)} %select_exponential_fusion) | copy-start | bytes 6291460 | tf_op jit(solution)/shard_map/while/body/eval_jaxpr/cond
  350.0 3.3 copy-start.3
  355.4 4.2 %copy-start.1 = (f32[4,2,256,256]{3,2,1,0:T(8,128)S(1)}, f32[4,2,256,256]{3,2,1,0:T(8,128)}, u32[]{:S(2)}) copy-start(f32[4,2,256,256]{3,2,1,0:T(8,128)} %select_exponential_fusion) | copy-start | bytes 6291460 | tf_op jit(solution)/shard_map/while/body/eval_jaxpr/cond
Sparse Core Ops, SparseCore 0:
  10.8 51.7 all-gather.4
  64.7 47.6 all-gather.6
  114.6 47.7 all-gather.8
  164.4 47.3 all-gather.10
  215.3 88.2 reduce-scatter.1
where the time goes:
time: 377 us; the launch traced here: 375 us
  waiting for transfers between devices  93.3 us (25%)
  blocking collectives  90.8 us (24%)
  matrix products  78.8 us (21%)
  local copies, waits for them, and re-layouts  58.8 us (16%)
  other arithmetic  27.1 us (7%)
  between operations  13.9 us (4%)
  loops' own time  11.7 us (3%)
    all_gather x1, blocking collectives, body(): all_stats = lax.all_gather(row_stats, 'sp', axis=0, tiled=True)  90.8 us
    all_gather x1, waiting for transfers between devices, body(): key_piece = lax.all_gather(key_heads, 'sp', axis=0, tiled=True)  46.7 us
    all_gather x1, waiting for transfers between devices, body(): value_piece = lax.all_gather(value_heads, 'sp', axis=0, tiled=True)  45.8 us
    dot_general x8, matrix products, block_grads(): jnp.einsum('qhmd,khmd->hmqk', query_split, key_split, preferred_element_t...  24.2 us
    dynamic_slice x25, local copies, waits for them, and re-layouts, body(): result, _ = lax.scan(visit, local_zero, blocks)  24 us
    unnamed x30, local copies, waits for them, and re-layouts  23.9 us
    dot_general x8, matrix products, block_grads(): jnp.einsum('hqk,qhe->khe', diff_weights, grad_blk, preferred_element_type...  19 us
    dot_general x8, matrix products, block_grads(): jnp.einsum('hmqk,qhmd->khmd', score_grad, query_split, preferred_element_...  18.2 us
  transfers between devices with their start and end apart: 5, of which 2 were waited for; matrix products, arithmetic and copies ran while one was open for 43% of the time, Pallas kernels for 0%

commit v1 on v0

v1 whole, which is shorter than its diff:
```python
import functools
import math

import jax
import jax.numpy as jnp
from jax import lax
from jax.experimental import pallas as pl
from jax.experimental.pallas import tpu as pltpu
from jax.sharding import PartitionSpec as P

EPSILON = 1e-05
LOG2E = math.log2(math.e)
F32 = jnp.float32
BF16 = jnp.bfloat16
MESH = pl.DeviceIdType.MESH


def dot_nn(a, b):
    return lax.dot_general(a, b, (((1,), (0,)), ((), ())), preferred_element_type=F32)


def dot_nt(a, b):
    return lax.dot_general(a, b, (((1,), (1,)), ((), ())), preferred_element_type=F32)


def dot_tn(a, b):
    return lax.dot_general(a, b, (((0,), (0,)), ((), ())), preferred_element_type=F32)


def prologue(heads, width, lam_ref, gain_ref, mo_ref, og_ref, lse_ref, q_ref, k_ref, v_ref,
             kv_ref, qg_ref, col_ref):
    kv_ref[0] = k_ref[...]
    kv_ref[1] = v_ref[...]
    qg_ref[0] = q_ref[...]
    for h in range(heads):
        at = slice(h * width, (h + 1) * width)
        first = mo_ref[:, at].astype(F32)
        second = mo_ref[:, heads * width + h * width : heads * width + (h + 1) * width].astype(F32)
        lam = lam_ref[h]
        combined = first - lam * second
        inverse = lax.rsqrt(jnp.mean(combined * combined, axis=-1, keepdims=True) + EPSILON)
        weighted = gain_ref[...] * og_ref[:, at].astype(F32)
        grad = (
            inverse * weighted
            - inverse**3 * combined * jnp.mean(combined * weighted, axis=-1, keepdims=True)
        ).astype(BF16)
        qg_ref[1, :, at] = grad
        wide = grad.astype(F32)
        lse = lse_ref[h] * LOG2E
        log_lam = jnp.log(jnp.full((1, 1), lam, F32)) * LOG2E
        col_ref[h, :, 0:1] = lse[:, 0:1]
        col_ref[h, :, 1:2] = lse[:, 1:2] - log_lam
        col_ref[h, :, 2:3] = jnp.sum(wide * first, axis=-1, keepdims=True)
        col_ref[h, :, 3:4] = jnp.sum(wide * second, axis=-1, keepdims=True)


def main_kernel(nsp, ntp, heads, width, lat, kv, qg, col, row,
                dq_out, dk_out, dv_out, wg_out,
                kvb, qgb, stb, dqb, latb, dq_acc, dk_acc, dv_acc,
                kv_s, qg_s, st_s, dq_s, kv_r, qg_r, st_r, dq_r,
                la_s, la_r, lb_s, lb_r, own_sem):
    nz = nsp // 2
    s = lax.axis_index("sp")
    t = lax.axis_index("tp")
    z, y = s // 2, lax.rem(s, 2)
    rows = kv.shape[1]
    part = rows // ntp
    slab = lat.shape[1] // nsp
    score_scale = (width // 2) ** (-0.5)
    exp_scale = score_scale * LOG2E

    barrier = pltpu.get_barrier_semaphore()
    for d in range(1, nsp):
        pl.semaphore_signal(barrier, inc=1, device_id={"sp": lax.rem(s + d, nsp)}, device_id_type=MESH)
    for d in range(1, ntp):
        pl.semaphore_signal(barrier, inc=1, device_id={"tp": lax.rem(t + d, ntp)}, device_id_type=MESH)
    pl.semaphore_wait(barrier, nsp - 1 + ntp - 1)

    def copy(src, dst, send, recv, to):
        return pltpu.make_async_remote_copy(
            src_ref=src, dst_ref=dst, send_sem=send, recv_sem=recv,
            device_id={"sp": to}, device_id_type=MESH)

    side = 2 * z + (1 - y)

    def kv_copy(block, lane, k, src=None):
        to = jnp.minimum(s + 2, nsp - 1) if lane == 0 else side
        return copy(kvb.at[block] if src is None else src, kvb.at[block],
                    kv_s.at[lane, k], kv_r.at[block], to)

    def qg_copies(block, lane, k, own=False):
        to = jnp.maximum(s - 2, 0) if lane == 0 else side
        return (
            copy(qg if own else qgb.at[block], qgb.at[block], qg_s.at[lane, k], qg_r.at[block], to),
            copy(row if own else stb.at[block], stb.at[block], st_s.at[lane, k], st_r.at[block], to),
        )

    @pl.when(z < nz - 1)
    def _():
        kv_copy(s, 0, 0, kv).start()

    @pl.when(z > 0)
    def _():
        for c in qg_copies(s, 0, 0, True):
            c.start()

    @pl.when(y == 0)
    def _():
        kv_copy(s, 1, 0, kv).start()

    @pl.when(y == 1)
    def _():
        for c in qg_copies(s, 1, 0, True):
            c.start()

    lane_id = lax.broadcasted_iota(jnp.int32, (1, width), 1)
    low = jnp.where(lane_id < width // 2, 1.0, 0.0).astype(BF16)
    high = jnp.where(lane_id < width // 2, 0.0, 1.0).astype(BF16)

    def split(x):
        return jnp.concatenate([x * low, x * high], axis=0)

    def query_side(kv_at, diagonal):
        def one(h, carry):
            at = pl.ds(pl.multiple_of(h * width, width), width)
            keys = split(kv_at[0, :, at])
            scores = dot_nt(qg[0, :, at], keys)
            mixed = dot_nt(qg[1, :, at], kv_at[1, :, at])
            stats = col[h]
            x1 = scores[:, :rows] * exp_scale - stats[:, 0:1]
            x2 = scores[:, rows:] * exp_scale - stats[:, 1:2]
            if diagonal:
                seen = (lax.broadcasted_iota(jnp.int32, (rows, rows), 1)
                        <= lax.broadcasted_iota(jnp.int32, (rows, rows), 0))
                x1 = jnp.where(seen, x1, -jnp.inf)
                x2 = jnp.where(seen, x2, -jnp.inf)
            g1 = (jnp.exp2(x1) * (mixed - stats[:, 2:3])).astype(BF16)
            g2 = (jnp.exp2(x2) * (stats[:, 3:4] - mixed)).astype(BF16)
            part_dq = dot_nn(jnp.concatenate([g1, g2], axis=1), keys)
            if diagonal:
                dq_acc[:, at] = part_dq
            else:
                dq_acc[:, at] += part_dq
            return carry
        lax.fori_loop(0, heads, one, 0)

    def key_side(qg_at, row_at, diagonal):
        def one(h, carry):
            at = pl.ds(pl.multiple_of(h * width, width), width)
            queries = split(qg_at[0, :, at])
            grads = qg_at[1, :, at]
            scores = dot_nt(kv[0, :, at], queries)
            mixed = dot_nt(kv[1, :, at], grads)
            stats = row_at[h]
            x1 = scores[:, :rows] * exp_scale - stats[0:1]
            x2 = scores[:, rows:] * exp_scale - stats[1:2]
            if diagonal:
                seen = (lax.broadcasted_iota(jnp.int32, (rows, rows), 0)
                        <= lax.broadcasted_iota(jnp.int32, (rows, rows), 1))
                x1 = jnp.where(seen, x1, -jnp.inf)
                x2 = jnp.where(seen, x2, -jnp.inf)
            p1 = jnp.exp2(x1)
            p2 = jnp.exp2(x2)
            g1 = (p1 * (mixed - stats[2:3])).astype(BF16)
            g2 = (p2 * (stats[3:4] - mixed)).astype(BF16)
            part_dv = dot_nn((p1 - p2).astype(BF16), grads)
            part_dk = dot_nn(jnp.concatenate([g1, g2], axis=1), queries)
            if diagonal:
                dv_acc[:, at] = part_dv
                dk_acc[:, at] = part_dk
            else:
                dv_acc[:, at] += part_dv
                dk_acc[:, at] += part_dk
            return carry
        lax.fori_loop(0, heads, one, 0)

    def lat_copy(d):
        to = lax.rem(s + d, nsp)
        mine = pl.ds(pl.multiple_of(t * part, part), part)
        return copy(lat.at[mine, pl.ds(pl.multiple_of(to * slab, slab), slab)],
                    latb.at[s, mine, :], la_s.at[d], la_r.at[d], to)

    def own_lat():
        return pltpu.make_async_copy(
            lat.at[pl.ds(pl.multiple_of(t * part, part), part), pl.ds(pl.multiple_of(s * slab, slab), slab)],
            latb.at[s, pl.ds(pl.multiple_of(t * part, part), part), :], own_sem)

    def share_copy(d):
        mine = pl.ds(pl.multiple_of(t * part, part), part)
        return pltpu.make_async_remote_copy(
            src_ref=latb.at[:, mine, :], dst_ref=latb.at[:, mine, :],
            send_sem=lb_s.at[d], recv_sem=lb_r.at[d],
            device_id={"tp": lax.rem(t + d, ntp)}, device_id_type=MESH)

    own_lat().start()
    query_side(kv, True)
    key_side(qg, row, True)
    for d in range(1, nsp):
        lat_copy(d).start()

    def step(k, carry):
        below, above = z - k, z + k
        has_below, has_above = below >= 0, above < nz
        kb = jnp.maximum(below, 0) * 2 + y
        qb = jnp.minimum(above, nz - 1) * 2 + y

        @pl.when(has_below)
        def _():
            kv_copy(kb, 0, 0).wait_recv()
            kv_copy(kb, 1, k).start()

        @pl.when(has_below & (z < nz - 1))
        def _():
            kv_copy(kb, 0, k).start()

        @pl.when(has_above)
        def _():
            for c in qg_copies(qb, 0, 0):
                c.wait_recv()
            for c in qg_copies(qb, 1, k):
                c.start()

        @pl.when(has_above & (z > 0))
        def _():
            for c in qg_copies(qb, 0, k):
                c.start()

        def turn(c, carry):
            dist = k - c
            other = jnp.where(c == 0, y, 1 - y)
            bz, qz = z - dist, z + dist
            use_kv = (bz >= 0) & (dist < nz) & ((dist > 0) | (y == 1))
            use_qg = (qz < nz) & (dist < nz) & ((dist > 0) | (y == 0))
            kblk = jnp.maximum(bz, 0) * 2 + other
            qblk = jnp.minimum(qz, nz - 1) * 2 + other

            @pl.when(use_kv)
            def _():
                @pl.when(c == 1)
                def _():
                    kv_copy(kblk, 1, 0).wait_recv()
                query_side(kvb.at[kblk], False)

            @pl.when(use_qg)
            def _():
                @pl.when(c == 1)
                def _():
                    for w in qg_copies(qblk, 1, 0):
                        w.wait_recv()
                key_side(qgb.at[qblk], stb.at[qblk], False)
            return carry
        lax.fori_loop(0, 2, turn, 0)
        return carry

    lax.fori_loop(1, nz + 1, step, 0)

    dq_out[...] = (dq_acc[...] * score_scale).astype(BF16)

    def dq_copy(block, lane, idx, src=None):
        to = (jnp.minimum(s + 2, nsp - 2 + y), jnp.maximum(s - 2, y), side)[lane]
        return copy(dqb.at[block] if src is None else src, dqb.at[block],
                    dq_s.at[lane, idx], dq_r.at[block], to)

    @pl.when(z < nz - 1)
    def _():
        dq_copy(s, 0, z, dq_out).start()

    @pl.when(z > 0)
    def _():
        dq_copy(s, 1, z, dq_out).start()

    dq_copy(s, 2, z, dq_out).start()

    dk_out[...] = (dk_acc[...] * score_scale).astype(BF16)
    dv_out[...] = dv_acc[...].astype(BF16)

    own_lat().wait()
    for d in range(1, nsp):
        lat_copy(d).wait_recv()
    for d in range(1, ntp):
        share_copy(d).start()
    for d in range(1, ntp):
        share_copy(d).wait_recv()

    wg_out[...] = dot_tn(latb[s], dq_out[...])

    def add_block(block):
        wg_out[...] += dot_tn(latb[block], dqb[block])

    def gather(k, carry):
        for lane, there, ok, more in (
            (0, z - k, z - k >= 0, z < nz - 1),
            (1, z + k, z + k < nz, z > 0),
        ):
            bz = jnp.clip(there, 0, nz - 1)
            block = bz * 2 + y

            @pl.when(ok)
            def _():
                dq_copy(block, lane, bz).wait_recv()
                dq_copy(block, 2, bz).start()

            @pl.when(ok & more)
            def _():
                dq_copy(block, lane, bz).start()

        def turn(c, carry):
            dist = jnp.where(c < 2, k, k - 1)
            up = lax.rem(c, 2)
            bz = jnp.where(up == 0, z - dist, z + dist)
            ok = (bz >= 0) & (bz < nz) & (dist < nz) & ((dist > 0) | (up == 0))
            other = jnp.where(c < 2, y, 1 - y)
            block = jnp.clip(bz, 0, nz - 1) * 2 + other

            @pl.when(ok)
            def _():
                @pl.when(c >= 2)
                def _():
                    dq_copy(block, 2, 0).wait_recv()
                add_block(block)
            return carry
        lax.fori_loop(0, 4, turn, 0)
        return carry

    lax.fori_loop(1, nz + 1, gather, 0)

    def drain(k, carry):
        below, above = z - k, z + k
        has_below, has_above = below >= 0, above < nz

        @pl.when(has_below & (z < nz - 1))
        def _():
            kv_copy(s, 0, k).wait_send()

        @pl.when(has_below & ((k > 0) | (y == 0)))
        def _():
            kv_copy(s, 1, k).wait_send()

        @pl.when(has_above & (z > 0))
        def _():
            for c in qg_copies(s, 0, k):
                c.wait_send()

        @pl.when(has_above & ((k > 0) | (y == 1)))
        def _():
            for c in qg_copies(s, 1, k):
                c.wait_send()

        @pl.when((k <= z) & (z < nz - 1))
        def _():
            dq_copy(s, 0, k).wait_send()

        @pl.when((k >= z) & (z > 0))
        def _():
            dq_copy(s, 1, k).wait_send()

        dq_copy(s, 2, k).wait_send()
        return carry

    lax.fori_loop(0, nz, drain, 0)
    for d in range(1, nsp):
        lat_copy(d).wait_send()
    for d in range(1, ntp):
        share_copy(d).wait_send()


def vmem():
    return pl.BlockSpec(memory_space=pltpu.VMEM)


def body(nsp, ntp, latents, query_heads, key_heads, value_heads, map_outputs, log_sums, out_grad,
         mix_lambda, norm_gain):
    rows, heads, width = query_heads.shape
    flat = (rows, heads * width)
    kv, qg, col = pl.pallas_call(
        functools.partial(prologue, heads, width),
        out_shape=(
            jax.ShapeDtypeStruct((2,) + flat, BF16),
            jax.ShapeDtypeStruct((2,) + flat, BF16),
            jax.ShapeDtypeStruct((heads, rows, 4), F32),
        ),
        in_specs=[pl.BlockSpec(memory_space=pltpu.SMEM)] + [vmem()] * 7,
        out_specs=(vmem(),) * 3,
        name="prologue",
    )(
        mix_lambda,
        norm_gain[None, :],
        map_outputs.reshape(rows, 2 * heads * width),
        out_grad.reshape(flat),
        jnp.transpose(log_sums, (1, 0, 2)),
        query_heads.reshape(flat),
        key_heads.reshape(flat),
        value_heads.reshape(flat),
    )
    row = jnp.transpose(col, (0, 2, 1))
    slab = latents.shape[1] // nsp
    nz = nsp // 2
    dma = pltpu.SemaphoreType.DMA
    dq, dk, dv, wg = pl.pallas_call(
        functools.partial(main_kernel, nsp, ntp, heads, width),
        out_shape=(
            jax.ShapeDtypeStruct(flat, BF16),
            jax.ShapeDtypeStruct(flat, BF16),
            jax.ShapeDtypeStruct(flat, BF16),
            jax.ShapeDtypeStruct((slab, heads * width), F32),
        ),
        in_specs=[vmem()] * 5,
        out_specs=(vmem(),) * 4,
        scratch_shapes=[
            pltpu.VMEM((nsp, 2) + flat, BF16),
            pltpu.VMEM((nsp, 2) + flat, BF16),
            pltpu.VMEM((nsp, heads, 4, rows), F32),
            pltpu.VMEM((nsp,) + flat, BF16),
            pltpu.VMEM((nsp, rows, slab), BF16),
            pltpu.VMEM(flat, F32),
            pltpu.VMEM(flat, F32),
            pltpu.VMEM(flat, F32),
            dma((2, nz)), dma((2, nz)), dma((2, nz)), dma((3, nz)),
            dma((nsp,)), dma((nsp,)), dma((nsp,)), dma((nsp,)),
            dma((nsp,)), dma((nsp,)), dma((ntp,)), dma((ntp,)),
            dma,
        ],
        compiler_params=pltpu.CompilerParams(collective_id=0, has_side_effects=True),
        name="main",
    )(latents, kv, qg, col, row)
    shape = (rows, heads, width)
    return dq.reshape(shape), dk.reshape(shape), dv.reshape(shape), wg


def solution(mesh):
    placed = (
        P("sp", None),
        P("sp", "tp", None),
        P("sp", "tp", None),
        P("sp", "tp", None),
        P("sp", None, "tp", None),
        P("sp", "tp", None),
        P("sp", "tp", None),
        P("tp"),
        P(),
    )
    return jax.shard_map(
        functools.partial(body, mesh.shape["sp"], mesh.shape["tp"]),
        mesh=mesh,
        in_specs=placed,
        out_specs=(P("sp", "tp", None), P("sp", "tp", None), P("sp", "tp", None), P("sp", "tp")),
        check_vma=False,
    )
```

time: 377 us -> 124 us (0.33)
  the two profiles are of different devices: /device:TPU:0 before, /device:TPU:1 now
where the time goes in v1:
time: 124 us
  Pallas kernels  108 us (87%)
  local copies, waits for them, and re-layouts  14.8 us (12%)
    pallas_call x1, Pallas kernels, body(): pl.pallas_call(functools.partial(main_kernel, nsp, ntp, heads, width), ou...  105 us
    reshape x3, local copies, waits for them, and re-layouts, body(): return (dq.reshape(shape), dk.reshape(shape), dv.reshape(shape), wg)  5.24 us
    pallas_call x1, Pallas kernels, body(): pl.pallas_call(functools.partial(prologue, heads, width), out_shape=(jax....  3.49 us
    unnamed x8, local copies, waits for them, and re-layouts  2.7 us

profile of v1, /device:TPU:1, one launch (start us, length us, event | category | flops | bytes accessed | tf_op | source)
XLA Modules:
  0.0 123.8 jit_solution(3977973740243571533)
XLA Ops:
  0.6 0.0 copy-start.1
  0.6 0.0 copy-start.2
  0.7 2.3 %reshape.32.mo_ref = bf16[256,1024]{1,0:T(8,128)(2,1)} reshape(bf16[256,2,4,128]{3,2,1,0:T(4,128)(2,1)} %param.13) | data formatting | bytes 1048576 | tf_op jit(solution)/shard_map/reshape | solution.py:388
  2.9 1.7 %copy.13 = f32[256,4,2]{2,0,1:T(8,128)} copy(f32[256,4,2]{0,2,1:T(2,128)} %param.14) | data formatting | bytes 16384 | tf_op args[5]
  4.6 1.9 %copy_bitcast_fusion.2 = (bf16[256,512]{1,0:T(8,128)(2,1)}, bf16[256,512]{1,0:T(8,128)(2,1)}) fusion(bf16[32,8,4,128]{3,2,1,0:T(4,128)(2,1)} %bitcast.16, bf16[32,8,4,128]{3,2,1,0:T(4,128)(2,1)} %bitcast.17), kind=kLoop, calls=%fused_computation.2 | loop fusion | bytes 1048576 | tf_op jit(solution)/shard_map/reshape | solution.py:391
  6.5 0.0 copy-done.1
  6.5 0.0 copy-done.2
  6.5 0.9 copy_bitcast_fusion
  7.4 3.5 %prologue.1 = (bf16[2,256,512]{2,1,0:T(8,128)(2,1)}, bf16[2,256,512]{2,1,0:T(8,128)(2,1)}, f32[4,256,4]{2,1,0:T(8,128)}) custom-call(f32[4]{0:T(128)} %lam_ref.1, f32[1,128]{1,0:T(1,128)} %bitcast.21, bf16[256,1024]{1,0:T(8,128)(2,1)} %reshape.32.mo_ref, bf16[256,512]{1,0:T(8,128)(2,1)} %get-tuple-element.21.og_ref, f32[4,256,2]{2,1,0:T(8,128)} %bitcast.15, ...), custom_call_target="tpu_custom_call" | custom-call | tf_op jit(solution)/shard_map/prologue/pallas_call | solution.py:375
  10.8 1.8 %copy.14 = f32[4,256,4]{1,2,0:T(4,128)} copy(f32[4,256,4]{2,1,0:T(8,128)} %get-tuple-element.13.col) | data formatting | bytes 32768 | tf_op jit(solution)/shard_map/prologue/pallas_call | solution.py:375
  12.7 104.9 %main.1 = (bf16[256,512]{1,0:T(8,128)(2,1)}, bf16[256,512]{1,0:T(8,128)(2,1)}, bf16[256,512]{1,0:T(8,128)(2,1)}, f32[512,512]{1,0:T(8,128)}) custom-call(bf16[256,4096]{1,0:T(8,128)(2,1)} %lat.1, bf16[2,256,512]{2,1,0:T(8,128)(2,1)} %get-tuple-element.11.kv, bf16[2,256,512]{2,1,0:T(8,128)(2,1)} %get-tuple-element.12.qg, f32[4,256,4]{2,1,0:T(8,128)} %get-tuple-element.13.col, ...), custom_call_target="tpu_custom_call" | custom-call | tf_op jit(solution)/shard_map/main/pallas_call | solution.py:399
  117.6 0.0 copy-start
  117.6 1.8 %reshape.37 = bf16[256,4,128]{2,1,0:T(4,128)(2,1)} reshape(bf16[256,512]{1,0:T(8,128)(2,1)} %get-tuple-element.14) | data formatting | bytes 524288 | tf_op jit(solution)/shard_map/reshape | solution.py:427
  119.4 1.7 %reshape.38 = bf16[256,4,128]{2,1,0:T(4,128)(2,1)} reshape(bf16[256,512]{1,0:T(8,128)(2,1)} %get-tuple-element.15) | data formatting | bytes 524288 | tf_op jit(solution)/shard_map/reshape | solution.py:427
  121.1 1.7 %reshape.39 = bf16[256,4,128]{2,1,0:T(4,128)(2,1)} reshape(bf16[256,512]{1,0:T(8,128)(2,1)} %get-tuple-element.16) | data formatting | bytes 524288 | tf_op jit(solution)/shard_map/reshape | solution.py:427
  122.9 0.0 copy-done
  122.9 1.0 copy.24
Async XLA Ops:
  0.6 5.9 %copy-start.1 = (bf16[256,4,128]{2,1,0:T(4,128)(2,1)S(1)}, bf16[256,4,128]{2,1,0:T(4,128)(2,1)}, u32[]{:S(2)}) copy-start(bf16[256,4,128]{2,1,0:T(4,128)(2,1)} %param.12) | copy-start | bytes 786436
  0.6 5.9 %copy-start.2 = (bf16[256,4,128]{2,1,0:T(4,128)(2,1)S(1)}, bf16[256,4,128]{2,1,0:T(4,128)(2,1)}, u32[]{:S(2)}) copy-start(bf16[256,4,128]{2,1,0:T(4,128)(2,1)} %param.11) | copy-start | bytes 786436
  117.6 5.3 %copy-start = (f32[512,512]{1,0:T(8,128)S(1)}, f32[512,512]{1,0:T(8,128)}, u32[]{:S(2)}) copy-start(f32[512,512]{1,0:T(8,128)} %get-tuple-element.29) | copy-start | bytes 3145732

commit v2 on v1

v2 whole, which is shorter than its diff:
```python
import functools
import math

import jax
import jax.numpy as jnp
from jax import lax
from jax.experimental import pallas as pl
from jax.experimental.pallas import tpu as pltpu
from jax.sharding import PartitionSpec as P

EPSILON = 1e-05
LOG2E = math.log2(math.e)
F32 = jnp.float32
BF16 = jnp.bfloat16
MESH = pl.DeviceIdType.MESH


def dot_nn(a, b):
    return lax.dot_general(a, b, (((1,), (0,)), ((), ())), preferred_element_type=F32)


def dot_nt(a, b):
    return lax.dot_general(a, b, (((1,), (1,)), ((), ())), preferred_element_type=F32)


def dot_tn(a, b):
    return lax.dot_general(a, b, (((0,), (0,)), ((), ())), preferred_element_type=F32)


def norm_backward(heads, width, lam_ref, gain_ref, mo_ref, og_ref, lse_ref, grad_ref, col_ref, row_ref):
    for h in range(heads):
        first = mo_ref[:, 0, h, :].astype(F32)
        second = mo_ref[:, 1, h, :].astype(F32)
        lam = lam_ref[h]
        combined = first - lam * second
        inverse = lax.rsqrt(jnp.mean(combined * combined, axis=-1, keepdims=True) + EPSILON)
        weighted = gain_ref[...] * og_ref[:, h, :].astype(F32)
        grad = (
            inverse * weighted
            - inverse**3 * combined * jnp.mean(combined * weighted, axis=-1, keepdims=True)
        ).astype(BF16)
        grad_ref[:, h * width : (h + 1) * width] = grad
        wide = grad.astype(F32)
        lse = lse_ref[h] * LOG2E
        log_lam = jnp.log(jnp.full((1, 1), lam, F32)) * LOG2E
        lane = lax.broadcasted_iota(jnp.int32, wide.shape, 1)
        stats = jnp.where(lane == 0, lse[:, 0:1], lse[:, 1:2] - log_lam)
        stats = jnp.where(lane == 2, jnp.sum(wide * first, axis=-1, keepdims=True), stats)
        stats = jnp.where(lane == 3, jnp.sum(wide * second, axis=-1, keepdims=True), stats)
        col_ref[h] = stats
        row_ref[h] = jnp.transpose(stats)[0:4]


def main_kernel(nsp, ntp, heads, width, lam, gain, lat, own_k, own_v, own_q, mo, og, lse,
                dq_out, dk_out, dv_out, wg_out,
                own_g, col, row, own_dq, kvb, qgb, stb, dqb, latb, dq_acc, dk_acc, dv_acc,
                kv_s, qg_s, st_s, dq_s, kv_r, qg_r, st_r, dq_r,
                la_s, la_r, lb_s, lb_r, own_sem):
    nz = nsp // 2
    s = lax.axis_index("sp")
    t = lax.axis_index("tp")
    z, y = s // 2, lax.rem(s, 2)
    rows = own_k.shape[0]
    part = rows // ntp
    slab = lat.shape[1] // nsp
    score_scale = (width // 2) ** (-0.5)
    exp_scale = score_scale * LOG2E

    barrier = pltpu.get_barrier_semaphore()
    for d in range(1, nsp):
        pl.semaphore_signal(barrier, inc=1, device_id={"sp": lax.rem(s + d, nsp)}, device_id_type=MESH)
    for d in range(1, ntp):
        pl.semaphore_signal(barrier, inc=1, device_id={"tp": lax.rem(t + d, ntp)}, device_id_type=MESH)
    pl.semaphore_wait(barrier, nsp - 1 + ntp - 1)

    def copy(src, dst, send, recv, to):
        return pltpu.make_async_remote_copy(
            src_ref=src, dst_ref=dst, send_sem=send, recv_sem=recv,
            device_id={"sp": to}, device_id_type=MESH)

    side = 2 * z + (1 - y)

    def kv_copy(block, lane, k, p, src=None):
        to = jnp.minimum(s + 2, nsp - 1) if lane == 0 else side
        return copy(kvb.at[block, p] if src is None else src, kvb.at[block, p],
                    kv_s.at[lane, p, k], kv_r.at[p, block], to)

    def qg_copy(block, lane, k, p, src=None):
        to = jnp.maximum(s - 2, 0) if lane == 0 else side
        return copy(qgb.at[block, p] if src is None else src, qgb.at[block, p],
                    qg_s.at[lane, p, k], qg_r.at[p, block], to)

    def st_copy(block, lane, k, src=None):
        to = jnp.maximum(s - 2, 0) if lane == 0 else side
        return copy(stb.at[block] if src is None else src, stb.at[block],
                    st_s.at[lane, k], st_r.at[block], to)

    for p, src in ((0, own_k), (1, own_v)):
        @pl.when(z < nz - 1)
        def _():
            kv_copy(s, 0, 0, p, src).start()

        @pl.when(y == 0)
        def _():
            kv_copy(s, 1, 0, p, src).start()

    @pl.when(z > 0)
    def _():
        qg_copy(s, 0, 0, 0, own_q).start()

    @pl.when(y == 1)
    def _():
        qg_copy(s, 1, 0, 0, own_q).start()

    norm_backward(heads, width, lam, gain, mo, og, lse, own_g, col, row)

    @pl.when(z > 0)
    def _():
        st_copy(s, 0, 0, row).start()
        qg_copy(s, 0, 0, 1, own_g).start()

    @pl.when(y == 1)
    def _():
        st_copy(s, 1, 0, row).start()
        qg_copy(s, 1, 0, 1, own_g).start()

    lane_id = lax.broadcasted_iota(jnp.int32, (1, width), 1)
    low = jnp.where(lane_id < width // 2, 1.0, 0.0).astype(BF16)
    high = jnp.where(lane_id < width // 2, 0.0, 1.0).astype(BF16)

    def split(x):
        return jnp.concatenate([x * low, x * high], axis=0)

    def query_side(k_at, v_at, diagonal):
        def one(h, carry):
            at = pl.ds(pl.multiple_of(h * width, width), width)
            keys = split(k_at[:, at])
            scores = dot_nt(own_q[:, at], keys)
            mixed = dot_nt(own_g[:, at], v_at[:, at])
            stats = col[h]
            x1 = scores[:, :rows] * exp_scale - stats[:, 0:1]
            x2 = scores[:, rows:] * exp_scale - stats[:, 1:2]
            if diagonal:
                seen = (lax.broadcasted_iota(jnp.int32, (rows, rows), 1)
                        <= lax.broadcasted_iota(jnp.int32, (rows, rows), 0))
                x1 = jnp.where(seen, x1, -jnp.inf)
                x2 = jnp.where(seen, x2, -jnp.inf)
            g1 = (jnp.exp2(x1) * (mixed - stats[:, 2:3])).astype(BF16)
            g2 = (jnp.exp2(x2) * (stats[:, 3:4] - mixed)).astype(BF16)
            part_dq = dot_nn(jnp.concatenate([g1, g2], axis=1), keys)
            if diagonal:
                dq_acc[:, at] = part_dq
            else:
                dq_acc[:, at] += part_dq
            return carry
        lax.fori_loop(0, heads, one, 0)

    def key_side(q_at, g_at, row_at, diagonal):
        def one(h, carry):
            at = pl.ds(pl.multiple_of(h * width, width), width)
            queries = split(q_at[:, at])
            grads = g_at[:, at]
            scores = dot_nt(own_k[:, at], queries)
            mixed = dot_nt(own_v[:, at], grads)
            stats = row_at[h]
            x1 = scores[:, :rows] * exp_scale - stats[0:1]
            x2 = scores[:, rows:] * exp_scale - stats[1:2]
            if diagonal:
                seen = (lax.broadcasted_iota(jnp.int32, (rows, rows), 0)
                        <= lax.broadcasted_iota(jnp.int32, (rows, rows), 1))
                x1 = jnp.where(seen, x1, -jnp.inf)
                x2 = jnp.where(seen, x2, -jnp.inf)
            p1 = jnp.exp2(x1)
            p2 = jnp.exp2(x2)
            g1 = (p1 * (mixed - stats[2:3])).astype(BF16)
            g2 = (p2 * (stats[3:4] - mixed)).astype(BF16)
            part_dv = dot_nn((p1 - p2).astype(BF16), grads)
            part_dk = dot_nn(jnp.concatenate([g1, g2], axis=1), queries)
            if diagonal:
                dv_acc[:, at] = part_dv
                dk_acc[:, at] = part_dk
            else:
                dv_acc[:, at] += part_dv
                dk_acc[:, at] += part_dk
            return carry
        lax.fori_loop(0, heads, one, 0)

    def lat_copy(d):
        to = lax.rem(s + d, nsp)
        mine = pl.ds(pl.multiple_of(t * part, part), part)
        return copy(lat.at[mine, pl.ds(pl.multiple_of(to * slab, slab), slab)],
                    latb.at[s, mine, :], la_s.at[d], la_r.at[d], to)

    def own_lat():
        return pltpu.make_async_copy(
            lat.at[pl.ds(pl.multiple_of(t * part, part), part), pl.ds(pl.multiple_of(s * slab, slab), slab)],
            latb.at[s, pl.ds(pl.multiple_of(t * part, part), part), :], own_sem)

    def share_copy(d):
        mine = pl.ds(pl.multiple_of(t * part, part), part)
        return pltpu.make_async_remote_copy(
            src_ref=latb.at[:, mine, :], dst_ref=latb.at[:, mine, :],
            send_sem=lb_s.at[d], recv_sem=lb_r.at[d],
            device_id={"tp": lax.rem(t + d, ntp)}, device_id_type=MESH)

    own_lat().start()
    query_side(own_k, own_v, True)
    key_side(own_q, own_g, row, True)
    for d in range(1, nsp):
        lat_copy(d).start()

    def step(k, carry):
        below, above = z - k, z + k
        has_below, has_above = below >= 0, above < nz
        kb = jnp.maximum(below, 0) * 2 + y
        qb = jnp.minimum(above, nz - 1) * 2 + y

        for p in range(2):
            @pl.when(has_below)
            def _():
                kv_copy(kb, 0, 0, p).wait_recv()
                kv_copy(kb, 1, k, p).start()

            @pl.when(has_below & (z < nz - 1))
            def _():
                kv_copy(kb, 0, k, p).start()

            @pl.when(has_above)
            def _():
                qg_copy(qb, 0, 0, p).wait_recv()
                qg_copy(qb, 1, k, p).start()
                if p == 0:
                    st_copy(qb, 0, 0).wait_recv()
                    st_copy(qb, 1, k).start()

            @pl.when(has_above & (z > 0))
            def _():
                qg_copy(qb, 0, k, p).start()
                if p == 0:
                    st_copy(qb, 0, k).start()

        def turn(c, carry):
            dist = k - c
            other = jnp.where(c == 0, y, 1 - y)
            bz, qz = z - dist, z + dist
            use_kv = (bz >= 0) & (dist < nz) & ((dist > 0) | (y == 1))
            use_qg = (qz < nz) & (dist < nz) & ((dist > 0) | (y == 0))
            kblk = jnp.maximum(bz, 0) * 2 + other
            qblk = jnp.minimum(qz, nz - 1) * 2 + other

            @pl.when(use_kv)
            def _():
                @pl.when(c == 1)
                def _():
                    for p in range(2):
                        kv_copy(kblk, 1, 0, p).wait_recv()
                query_side(kvb.at[kblk, 0], kvb.at[kblk, 1], False)

            @pl.when(use_qg)
            def _():
                @pl.when(c == 1)
                def _():
                    for p in range(2):
                        qg_copy(qblk, 1, 0, p).wait_recv()
                    st_copy(qblk, 1, 0).wait_recv()
                key_side(qgb.at[qblk, 0], qgb.at[qblk, 1], stb.at[qblk], False)
            return carry
        lax.fori_loop(0, 2, turn, 0)
        return carry

    lax.fori_loop(1, nz + 1, step, 0)

    own_dq[...] = (dq_acc[...] * score_scale).astype(BF16)
    half = rows // 2

    def dq_copy(block, lane, idx, p, own=False):
        to = (jnp.minimum(s + 2, nsp - 2 + y), jnp.maximum(s - 2, y), side)[lane]
        at = pl.ds(p * half, half)
        return copy(own_dq.at[at] if own else dqb.at[block, at], dqb.at[block, at],
                    dq_s.at[lane, p, idx], dq_r.at[p, block], to)

    for p in range(2):
        @pl.when(z < nz - 1)
        def _():
            dq_copy(s, 0, z, p, True).start()

        @pl.when(z > 0)
        def _():
            dq_copy(s, 1, z, p, True).start()

        dq_copy(s, 2, z, p, True).start()

    for h in range(heads):
        at = slice(h * width, (h + 1) * width)
        dq_out[:, h, :] = own_dq[:, at]
        dk_out[:, h, :] = (dk_acc[:, at] * score_scale).astype(BF16)
        dv_out[:, h, :] = dv_acc[:, at].astype(BF16)

    own_lat().wait()
    for d in range(1, nsp):
        lat_copy(d).wait_recv()
    for d in range(1, ntp):
        share_copy(d).start()
    for d in range(1, ntp):
        share_copy(d).wait_recv()

    wg_out[...] = dot_tn(latb[s], own_dq[...])

    def add_block(block):
        wg_out[...] += dot_tn(latb[block], dqb[block])

    def gather(k, carry):
        for p in range(2):
            for lane, there, ok, more in (
                (0, z - k, z - k >= 0, z < nz - 1),
                (1, z + k, z + k < nz, z > 0),
            ):
                bz = jnp.clip(there, 0, nz - 1)
                block = bz * 2 + y

                @pl.when(ok)
                def _():
                    dq_copy(block, lane, bz, p).wait_recv()
                    dq_copy(block, 2, bz, p).start()

                @pl.when(ok & more)
                def _():
                    dq_copy(block, lane, bz, p).start()

        def turn(c, carry):
            dist = jnp.where(c < 2, k, k - 1)
            up = lax.rem(c, 2)
            bz = jnp.where(up == 0, z - dist, z + dist)
            ok = (bz >= 0) & (bz < nz) & (dist < nz) & ((dist > 0) | (up == 0))
            other = jnp.where(c < 2, y, 1 - y)
            block = jnp.clip(bz, 0, nz - 1) * 2 + other

            @pl.when(ok)
            def _():
                @pl.when(c >= 2)
                def _():
                    for p in range(2):
                        dq_copy(block, 2, 0, p).wait_recv()
                add_block(block)
            return carry
        lax.fori_loop(0, 4, turn, 0)
        return carry

    lax.fori_loop(1, nz + 1, gather, 0)

    def drain(k, carry):
        below, above = z - k, z + k
        has_below, has_above = below >= 0, above < nz

        for p in range(2):
            @pl.when(has_below & (z < nz - 1))
            def _():
                kv_copy(s, 0, k, p).wait_send()

            @pl.when(has_below & ((k > 0) | (y == 0)))
            def _():
                kv_copy(s, 1, k, p).wait_send()

            @pl.when(has_above & (z > 0))
            def _():
                qg_copy(s, 0, k, p).wait_send()
                if p == 0:
                    st_copy(s, 0, k).wait_send()

            @pl.when(has_above & ((k > 0) | (y == 1)))
            def _():
                qg_copy(s, 1, k, p).wait_send()
                if p == 0:
                    st_copy(s, 1, k).wait_send()

            @pl.when((k <= z) & (z < nz - 1))
            def _():
                dq_copy(s, 0, k, p).wait_send()

            @pl.when((k >= z) & (z > 0))
            def _():
                dq_copy(s, 1, k, p).wait_send()

            dq_copy(s, 2, k, p).wait_send()
        return carry

    lax.fori_loop(0, nz, drain, 0)
    for d in range(1, nsp):
        lat_copy(d).wait_send()
    for d in range(1, ntp):
        share_copy(d).wait_send()


def vmem():
    return pl.BlockSpec(memory_space=pltpu.VMEM)


def body(nsp, ntp, latents, query_heads, key_heads, value_heads, map_outputs, log_sums, out_grad,
         mix_lambda, norm_gain):
    rows, heads, width = query_heads.shape
    flat = (rows, heads * width)
    slab = latents.shape[1] // nsp
    nz = nsp // 2
    dma = pltpu.SemaphoreType.DMA
    dq, dk, dv, wg = pl.pallas_call(
        functools.partial(main_kernel, nsp, ntp, heads, width),
        out_shape=(
            jax.ShapeDtypeStruct(query_heads.shape, BF16),
            jax.ShapeDtypeStruct(query_heads.shape, BF16),
            jax.ShapeDtypeStruct(query_heads.shape, BF16),
            jax.ShapeDtypeStruct((slab, heads * width), F32),
        ),
        in_specs=[pl.BlockSpec(memory_space=pltpu.SMEM)] + [vmem()] * 8,
        out_specs=(vmem(),) * 4,
        scratch_shapes=[
            pltpu.VMEM(flat, BF16),
            pltpu.VMEM((heads, rows, width), F32),
            pltpu.VMEM((heads, 4, rows), F32),
            pltpu.VMEM(flat, BF16),
            pltpu.VMEM((nsp, 2) + flat, BF16),
            pltpu.VMEM((nsp, 2) + flat, BF16),
            pltpu.VMEM((nsp, heads, 4, rows), F32),
            pltpu.VMEM((nsp,) + flat, BF16),
            pltpu.VMEM((nsp, rows, slab), BF16),
            pltpu.VMEM(flat, F32),
            pltpu.VMEM(flat, F32),
            pltpu.VMEM(flat, F32),
            dma((2, 2, nz)), dma((2, 2, nz)), dma((2, nz)), dma((3, 2, nz)),
            dma((2, nsp)), dma((2, nsp)), dma((nsp,)), dma((2, nsp)),
            dma((nsp,)), dma((nsp,)), dma((ntp,)), dma((ntp,)),
            dma,
        ],
        compiler_params=pltpu.CompilerParams(collective_id=0, has_side_effects=True),
        name="main",
    )(
        mix_lambda,
        norm_gain[None, :],
        latents,
        key_heads.reshape(flat),
        value_heads.reshape(flat),
        query_heads.reshape(flat),
        map_outputs,
        out_grad,
        jnp.transpose(log_sums, (1, 0, 2)),
    )
    return dq, dk, dv, wg


def solution(mesh):
    placed = (
        P("sp", None),
        P("sp", "tp", None),
        P("sp", "tp", None),
        P("sp", "tp", None),
        P("sp", None, "tp", None),
        P("sp", "tp", None),
        P("sp", "tp", None),
        P("tp"),
        P(),
    )
    return jax.shard_map(
        functools.partial(body, mesh.shape["sp"], mesh.shape["tp"]),
        mesh=mesh,
        in_specs=placed,
        out_specs=(P("sp", "tp", None), P("sp", "tp", None), P("sp", "tp", None), P("sp", "tp")),
        check_vma=False,
    )
```

time: 124 us -> 116 us (0.935)
  Pallas kernels: 108 us -> 104 us
  local copies, waits for them, and re-layouts: 14.8 us -> 11.6 us
    reshape x5 -> x0, local copies, waits for them, and re-layouts: 8.34 us -> none  [the longest x3 5.24 us: body(): return (dq.reshape(shape), dk.reshape(shape), dv.reshape(shape), wg)]
    unnamed x8, local copies, waits for them, and re-layouts: 2.7 us -> 9.7 us
    pallas_call x1 -> x0, Pallas kernels: 3.49 us -> none  [body(): pl.pallas_call(functools.partial(prologue, heads, width), out_shape=(jax....]
    pallas_call x1 -> x0, local copies, waits for them, and re-layouts: 1.83 us -> none  [body(): pl.pallas_call(functools.partial(prologue, heads, width), out_shape=(jax....]
    pallas_call x1, Pallas kernels: 105 us -> 104 us  [body(): pl.pallas_call(functools.partial(main_kernel, nsp, ntp, heads, width), ou...]
where the time goes in v2:
time: 116 us
  Pallas kernels  104 us (90%)
  local copies, waits for them, and re-layouts  11.6 us (10%)
    pallas_call x1, Pallas kernels, body(): pl.pallas_call(functools.partial(main_kernel, nsp, ntp, heads, width), ou...  104 us
    unnamed x8, local copies, waits for them, and re-layouts  9.7 us

profile of v2, /device:TPU:1, one launch (start us, length us, event | category | flops | bytes accessed | tf_op | source)
XLA Modules:
  0.0 115.9 jit_solution(17533509706725338349)
XLA Ops:
  0.6 1.7 %copy.20 = bf16[32,8,4,128]{3,1,2,0:T(8,128)(2,1)} copy(bf16[32,8,4,128]{3,2,1,0:T(4,128)(2,1)} %bitcast.14) | data formatting | bytes 524288
  2.3 1.7 %copy.13 = f32[256,4,2]{2,0,1:T(8,128)} copy(f32[256,4,2]{0,2,1:T(2,128)} %param.14) | data formatting | bytes 16384 | tf_op args[5]
  4.0 1.9 %copy_bitcast_fusion = (bf16[256,512]{1,0:T(8,128)(2,1)}, bf16[256,512]{1,0:T(8,128)(2,1)}) fusion(bf16[32,8,4,128]{3,2,1,0:T(4,128)(2,1)} %bitcast.15, bf16[32,8,4,128]{3,2,1,0:T(4,128)(2,1)} %bitcast.16), kind=kLoop, calls=%fused_computation | loop fusion | bytes 1048576 | tf_op jit(solution)/shard_map/reshape | solution.py:441
  5.9 103.7 %main.1 = (bf16[256,4,128]{2,1,0:T(4,128)(2,1)}, bf16[256,4,128]{2,1,0:T(4,128)(2,1)}, bf16[256,4,128]{2,1,0:T(4,128)(2,1)}, f32[512,512]{1,0:T(8,128)}) custom-call(f32[4]{0:T(128)} %lam.1, f32[1,128]{1,0:T(1,128)} %bitcast.17, bf16[256,4096]{1,0:T(8,128)(2,1)} %lat.1, bf16[256,512]{1,0:T(8,128)(2,1)} %bitcast.13, bf16[256,512]{1,0:T(8,128)(2,1)} %get-tuple-element.5.own_v, ...), custom_call_target="tpu_custom_call" | custom-call | tf_op jit(solution)/shard_map/main/pallas_call | solution.py:405
  109.6 0.0 copy-start
  109.6 1.8 %copy.25 = bf16[256,4,128]{2,1,0:T(4,128)(2,1)} copy(bf16[256,4,128]{2,1,0:T(4,128)(2,1)} %get-tuple-element.10) | data formatting | bytes 524288
  111.4 1.7 %copy.26 = bf16[256,4,128]{2,1,0:T(4,128)(2,1)} copy(bf16[256,4,128]{2,1,0:T(4,128)(2,1)} %get-tuple-element.11) | data formatting | bytes 524288
  113.2 1.7 %copy.27 = bf16[256,4,128]{2,1,0:T(4,128)(2,1)} copy(bf16[256,4,128]{2,1,0:T(4,128)(2,1)} %get-tuple-element.12) | data formatting | bytes 524288
  114.9 0.0 copy-done
  114.9 1.0 copy.28
Async XLA Ops:
  109.6 5.3 %copy-start = (f32[512,512]{1,0:T(8,128)S(1)}, f32[512,512]{1,0:T(8,128)}, u32[]{:S(2)}) copy-start(f32[512,512]{1,0:T(8,128)} %get-tuple-element.13) | copy-start | bytes 3145732
